TPU v7x, 32 devices: a whole 2x2x4 slice. The times are simulated.
32 devices in a mesh: grp: 2 (over x), ep: 16 (over z, y, core).
Axes of the slice: x: 2, y: 2, z: 4, core: 2. Of those that a mesh axis runs over, the one named last changes fastest.
Arguments:
- tokens: bfloat16 [128, 2048], P(('grp', 'ep')), parts along dimension 0, may hold values from -30 to 30
- state: float32 [128, 16, 128, 128], P(('grp', 'ep')), parts along dimension 0, may hold values from -6 to 6
- route_ids: int32 [128, 2], P(('grp', 'ep')), parts along dimension 0, may hold values from 0 to 3, all different within a row; in each aligned block of 4 rows (0 to 3, 4 to 7, ...) at most 3 rows name the same one
- route_weights: bfloat16 [128, 2], P(('grp', 'ep')), parts along dimension 0, may hold values from 0.099609375 to 1
- norm_mix: float32 [2048], replicated, may hold values from 0.1 to 1.9
- w_query: bfloat16 [2048, 2048], P(None, 'ep'), may hold values from -0.125 to 0.125
- w_forget: bfloat16 [2048, 2048], P(None, 'ep'), may hold values from -0.125 to 0.125
- w_input: bfloat16 [2048, 2048], P(None, 'ep'), may hold values from -0.125 to 0.125
- w_gate: bfloat16 [2048, 2048], P(None, 'ep'), may hold values from -0.125 to 0.125
- lower_bound: float32 [2048], replicated, may hold values from 0.05 to 0.9
- head_gain: float32 [128], replicated, may hold values from 0.1 to 1.9
- w_out: bfloat16 [2048, 2048], P(None, 'ep'), may hold values from -0.125 to 0.125
- norm_ffn: float32 [2048], replicated, may hold values from 0.1 to 1.9
- expert_gate: bfloat16 [2048, 28672], P(None, 'ep'), may hold values from -0.125 to 0.125
- expert_up: bfloat16 [2048, 28672], P(None, 'ep'), may hold values from -0.125 to 0.125
- expert_down: bfloat16 [28672, 2048], P('ep'), may hold values from -0.0625 to 0.0625
Outputs:
- layer_out: bfloat16 [128, 2048], P(('grp', 'ep')), parts along dimension 0
- new_state: float32 [128, 16, 128, 128], P(('grp', 'ep')), parts along dimension 0
There are 2 independent parts, one for each index of `grp`. A program takes and returns all parts, laid end to end along the dimension named above; an argument that names none is the same for every part. Nothing has to cross between parts.
Inputs may be any that keep to these rules, and one draw needn't show every extreme that they name: `route_ids`: each row names 2 different experts; the rows of one device name no expert more than 3 times, and some device names one exactly 3 times.
All inputs are finite; a program needn't handle non-finite values.
Results may differ from a plain program's by a relative error of at most 0.008.
Values may be sent and summed in bfloat16 or wider, within the bound.
No kernel may reach another device: no remote copies, remote signals or barrier semaphores. Data moves between devices by JAX's collectives and lax.ppermute only.
A program may use at most 64 MiB of HBM per device.

v0:
```python
import jax
import jax.numpy as jnp
from jax import lax
from jax.sharding import PartitionSpec as P

FF = 7168
EXPERTS = 4
CAP = 3
epsilon = 1e-06


def rms_scale(values, gain):
    return values * lax.rsqrt(jnp.mean(values * values, axis=-1, keepdims=True) + epsilon) * gain


def mixer_state(projected, state, lower_bound, head_gain):
    query_raw = projected[0].astype(jnp.float32)
    forget_raw = projected[1].astype(jnp.float32)
    input_raw = projected[2].astype(jnp.float32)
    gate_raw = projected[3].astype(jnp.float32)
    seq_rows = state.shape[0]
    heads = state.shape[1]
    head_dim = state.shape[2]
    head_shape = (seq_rows, heads, head_dim)
    log_forget = jnp.logaddexp(
        jnp.log(lower_bound), jnp.log1p(-lower_bound) + jax.nn.log_sigmoid(forget_raw)
    )
    key_vec = (1.0 - lower_bound) * jax.nn.sigmoid(-forget_raw)
    query_vec = jax.nn.silu(query_raw) * head_dim ** (-0.5)
    new_state = (
        jnp.exp(log_forget).reshape(head_shape)[..., None] * state
        + key_vec.reshape(head_shape)[..., None] * input_raw.reshape(head_shape)[:, :, None, :]
    )
    read_out = jnp.einsum(
        "thk,thkv->thv", query_vec.reshape(head_shape), new_state, precision=lax.Precision.HIGHEST
    )
    mixed = rms_scale(read_out, head_gain) * jax.nn.silu(gate_raw.reshape(head_shape))
    return (mixed.reshape(seq_rows, heads * head_dim).astype(jnp.bfloat16), new_state)


def local(
    tokens,
    state,
    route_ids,
    route_weights,
    norm_mix,
    w_query,
    w_forget,
    w_input,
    w_gate,
    lower_bound,
    head_gain,
    w_out,
    norm_ffn,
    expert_gate,
    expert_up,
    expert_down,
):
    model_width = tokens.shape[1]
    expert_group = FF // expert_gate.shape[1]
    all_tokens, all_ids, all_weights = (
        lax.all_gather(tokens, "ep", axis=0, tiled=True),
        lax.all_gather(route_ids, "ep", axis=0, tiled=True),
        lax.all_gather(route_weights, "ep", axis=0, tiled=True),
    )
    normed = rms_scale(all_tokens.astype(jnp.float32), norm_mix).astype(jnp.bfloat16)
    projected = jnp.stack(
        [
            jnp.dot(normed, weight, preferred_element_type=jnp.float32).astype(jnp.bfloat16)
            for weight in (w_query, w_forget, w_input, w_gate)
        ]
    )
    owned = lax.all_to_all(projected, "ep", split_axis=1, concat_axis=2, tiled=True)
    mixed, new_state = mixer_state(owned, state, lower_bound, head_gain)
    mixer_cols = jnp.dot(
        lax.all_gather(mixed, "ep", axis=0, tiled=True), w_out, preferred_element_type=jnp.float32
    ).astype(jnp.bfloat16)
    mixer_rows = lax.all_to_all(mixer_cols, "ep", split_axis=0, concat_axis=1, tiled=True)
    middle = tokens.astype(jnp.float32) + mixer_rows.astype(jnp.float32)
    normed_two = rms_scale(middle, norm_ffn).astype(jnp.bfloat16)
    matches = (route_ids[:, :, None] == jnp.arange(EXPERTS, dtype=jnp.int32)[None, None, :]).astype(
        jnp.int32
    )
    hit_mask = jnp.sum(matches, axis=1)
    combined = jnp.sum(
        route_weights.astype(jnp.float32)[:, :, None] * matches.astype(jnp.float32), axis=1
    )
    slot_rank = jnp.cumsum(hit_mask, axis=0) - hit_mask
    slot_ids = jnp.arange(CAP, dtype=jnp.int32)
    placing = (
        (slot_rank.T[:, None, :] == slot_ids[None, :, None]) & (hit_mask.T[:, None, :] > 0)
    ).astype(jnp.float32)
    outgoing = jnp.einsum(
        "ect,td->ecd", placing.astype(jnp.bfloat16), normed_two, preferred_element_type=jnp.float32
    ).astype(jnp.bfloat16)
    outgoing = jnp.repeat(outgoing, expert_group, axis=0)
    arrived = lax.all_to_all(outgoing, "ep", split_axis=0, concat_axis=0, tiled=True)
    gate_act = jnp.einsum("scd,df->scf", arrived, expert_gate, preferred_element_type=jnp.float32)
    up_act = jnp.einsum("scd,df->scf", arrived, expert_up, preferred_element_type=jnp.float32)
    hidden = (jax.nn.silu(gate_act) * up_act).astype(jnp.bfloat16)
    partial_rows = jnp.einsum(
        "scf,fd->scd", hidden, expert_down, preferred_element_type=jnp.float32
    )
    returned = lax.all_to_all(
        partial_rows.astype(jnp.bfloat16), "ep", split_axis=0, concat_axis=0, tiled=True
    ).astype(partial_rows.dtype)
    summed = jnp.sum(
        returned.reshape(EXPERTS, expert_group, returned.shape[1], model_width), axis=1
    )
    expert_total = jnp.einsum(
        "ect,ecd->td", placing * combined.T[:, None, :], summed, precision=lax.Precision.HIGHEST
    )
    layer_out = (middle + expert_total).astype(jnp.bfloat16)
    return (layer_out, new_state)


def solution(mesh):
    return jax.shard_map(
        local,
        mesh=mesh,
        in_specs=(
            P(("grp", "ep"), None),
            P(("grp", "ep"), None, None, None),
            P(("grp", "ep"), None),
            P(("grp", "ep"), None),
            P(),
            P(None, "ep"),
            P(None, "ep"),
            P(None, "ep"),
            P(None, "ep"),
            P(),
            P(),
            P(None, "ep"),
            P(),
            P(None, "ep"),
            P(None, "ep"),
            P("ep", None),
        ),
        out_specs=(P(("grp", "ep"), None), P(("grp", "ep"), None, None, None)),
        check_vma=False,
    )
```

profile of v0, /device:TPU:0, one launch (start us, length us, event | category | flops | bytes accessed | tf_op | source)
XLA Modules:
  0.0 121.8 jit_solution(15939425539012757206)
XLA Ops:
  0.6 0.0 copy-start
  0.6 24.2 %all-gather = bf16[16,4,2048]{2,1,0:T(4,128)(2,1)S(1)} all-gather(bf16[1,4,2048]{2,1,0:T(4,128)(2,1)} %bitcast.138), channel_id=1, replica_groups=mesh['grp'=2,'ep'=16] {'ep'}, dimensions={0}, use_global_device_ids=true | all-gather | bytes 278528 | tf_op jit(solution)/shard_map/all_gather | solution.py:62
  24.9 0.1 multiply_reduce_fusion
  25.0 0.8 multiply_convert_fusion
  25.9 0.0 copy-done
  25.9 0.2 fusion.17
  26.1 1.3 %fusion.18 = bf16[1,64,128]{2,1,0:T(8,128)(2,1)S(1)} fusion(bf16[64,2048]{1,0:T(8,128)(2,1)S(1)} %multiply_convert_fusion, bf16[2048,128]{1,0:T(8,128)(2,1)} %param.22), kind=kOutput, calls=%fused_computation.20 | convolution fusion | flops 33562624 | bytes 802816 | tf_op jit(solution)/shard_map/dot_general | solution.py:69
  27.4 1.3 %fusion.19 = bf16[1,64,128]{2,1,0:T(8,128)(2,1)S(1)} fusion(bf16[64,2048]{1,0:T(8,128)(2,1)S(1)} %multiply_convert_fusion, bf16[2048,128]{1,0:T(8,128)(2,1)} %param.23), kind=kOutput, calls=%fused_computation.21 | convolution fusion | flops 33562624 | bytes 802816 | tf_op jit(solution)/shard_map/dot_general | solution.py:69
  28.7 0.0 copy-start.5
  28.7 1.3 %fusion.20 = bf16[1,64,128]{2,1,0:T(8,128)(2,1)S(1)} fusion(bf16[64,2048]{1,0:T(8,128)(2,1)S(1)} %multiply_convert_fusion, bf16[2048,128]{1,0:T(8,128)(2,1)} %param.24), kind=kOutput, calls=%fused_computation.22 | convolution fusion | flops 33562624 | bytes 802816 | tf_op jit(solution)/shard_map/dot_general | solution.py:69
  30.0 0.0 copy-start.2
  30.0 0.7 copy.66
  30.7 3.5 %all-to-all-start = ((bf16[4,64,128]{2,0,1:T(4,128)(2,1)}), bf16[4,64,128]{2,0,1:T(4,128)(2,1)S(1)}, u32[]{:S(2)}, u32[]{:S(2)}) async-start(bf16[4,64,128]{2,0,1:T(4,128)(2,1)} %copy.66), calls=%async_computation | async-start | bytes 131072 | tf_op jit(solution)/shard_map/all_to_all | solution.py:73
  34.2 0.7 log_bitcast_fusion
  34.9 0.8 convert_reduce_fusion.1
  35.7 5.3 %all-to-all-done = bf16[4,64,128]{2,0,1:T(4,128)(2,1)S(1)} async-done(((bf16[4,64,128]{2,0,1:T(4,128)(2,1)}), bf16[4,64,128]{2,0,1:T(4,128)(2,1)S(1)}, u32[]{:S(2)}, u32[]{:S(2)}) %all-to-all-start) | async-done | bytes 65568 | tf_op jit(solution)/shard_map/all_to_all | solution.py:73
  41.1 0.0 copy-start.3
  41.1 0.0 copy-start.6
  41.1 0.1 select_exponential_fusion
  41.2 4.4 %multiply_add_fusion = f32[4,16,128,128]{3,2,1,0:T(8,128)S(1)} fusion(f32[4,16,128,128]{3,2,1,0:T(8,128)} %param.17, f32[4,16,128]{2,1,0:T(8,128)S(1)} %fusion.57, f32[4,16,128]{2,1,0:T(8,128)S(1)} %get-tuple-element.3, f32[4,16,128]{2,1,0:T(8,128)S(1)} %get-tuple-element.2), kind=kLoop, calls=%fused_computation.6 | loop fusion | flops 3145728 | bytes 8486912 | tf_op jit(solution)/shard_map/add | solution.py:31
  45.6 0.0 copy-start.1
  45.6 2.0 %copy-done.1 = f32[4,16,128,128]{3,2,1,0:T(8,128)} copy-done((f32[4,16,128,128]{3,2,1,0:T(8,128)}, f32[4,16,128,128]{3,2,1,0:T(8,128)S(1)}, u32[]{:S(2)}) %copy-start.1) | copy-done | bytes 4194328
  47.6 3.6 %fusion.73 = f32[4,16,1,128]{3,2,1,0:T(1,128)S(1)} fusion(f32[4,16,128,1]{2,3,1,0:T(1,128)S(1)} %bitcast.137, f32[4,16,128,128]{3,2,1,0:T(8,128)S(1)} %multiply_add_fusion), kind=kOutput, calls=%fused_computation.103 | convolution fusion | flops 12582912 | bytes 4259840 | tf_op jit(solution)/shard_map/thk,thkv->thv/dot_general | solution.py:34
  51.3 0.1 multiply_reduce_fusion.2
  51.4 0.0 copy-done.5
  51.4 0.1 fusion.54
  51.5 18.4 %all-gather.1 = bf16[16,4,2048]{2,1,0:T(4,128)(2,1)S(1)} all-gather(bf16[1,4,2048]{2,1,0:T(4,128)(2,1)S(1)} %reshape.164), channel_id=1, replica_groups=mesh['grp'=2,'ep'=16] {'ep'}, dimensions={0}, use_global_device_ids=true | all-gather | bytes 278528 | tf_op jit(solution)/shard_map/all_gather | solution.py:76
  69.9 0.1 reshape.165
  70.0 0.0 copy-done.2
  70.0 0.8 convolution_convert_fusion.1
  70.8 3.5 %all-to-all-start.1 = ((bf16[16,4,128]{2,1,0:T(4,128)(2,1)}), bf16[16,4,128]{2,1,0:T(4,128)(2,1)S(1)}, u32[]{:S(2)}, u32[]{:S(2)}) async-start(bf16[16,4,128]{2,1,0:T(4,128)(2,1)} %bitcast.21), calls=%async_computation.1 | async-start | bytes 32768 | tf_op jit(solution)/shard_map/all_to_all | solution.py:78
  74.3 6.5 %all-to-all-done.1 = bf16[16,4,128]{2,1,0:T(4,128)(2,1)S(1)} async-done(((bf16[16,4,128]{2,1,0:T(4,128)(2,1)}), bf16[16,4,128]{2,1,0:T(4,128)(2,1)S(1)}, u32[]{:S(2)}, u32[]{:S(2)}) %all-to-all-start.1) | async-done | bytes 16416 | tf_op jit(solution)/shard_map/all_to_all | solution.py:78
  80.8 0.0 copy-done.3
  80.8 0.1 multiply_reduce_fusion.1
  80.9 0.2 convolution_convert_fusion
  81.2 0.1 broadcast_in_dim.2
  81.3 12.6 %all_to_all.38 = bf16[16,3,2048]{2,1,0:T(4,128)(2,1)S(1)} all-to-all(bf16[16,3,2048]{2,1,0:T(4,128)(2,1)S(1)} %bitcast.130), channel_id=1, replica_groups=mesh['grp'=2,'ep'=16] {'ep'}, dimensions={0} | all-to-all | bytes 393216 | tf_op jit(solution)/shard_map/all_to_all | solution.py:97
  93.9 4.5 %fusion.4 = f32[16,3,1792]{2,0,1:T(8,128)S(1)} fusion(bf16[2048,1792]{1,0:T(8,128)(2,1)} %param.29, bf16[16,3,2048]{2,1,0:T(4,128)(2,1)S(1)} %all_to_all.38), kind=kOutput, calls=%fused_computation.4 | convolution fusion | flops 352321536 | bytes 7880704 | tf_op jit(solution)/shard_map/scd,df->scf/dot_general | solution.py:98
  98.4 0.0 copy-start.7
  98.5 0.0 copy-start.4
  98.5 7.9 %fusion.12 = bf16[16,3,2048]{2,0,1:T(8,128)(2,1)S(1)} fusion(bf16[1792,2048]{1,0:T(8,128)(2,1)} %param.31, bf16[2048,1792]{1,0:T(8,128)(2,1)} %param.30, f32[16,3,1792]{2,0,1:T(8,128)S(1)} %fusion.4, bf16[16,3,2048]{2,1,0:T(4,128)(2,1)S(1)} %all_to_all.38), kind=kOutput, calls=%fused_computation.9 | convolution fusion | flops 705257472 | bytes 15417344 | tf_op jit(solution)/shard_map/scf,fd->scd/dot_general | solution.py:101
  106.4 0.9 copy.73
  107.2 3.5 %all-to-all-start.3 = ((bf16[16,3,2048]{2,1,0:T(4,128)(2,1)}), bf16[16,3,2048]{2,1,0:T(4,128)(2,1)S(1)}, u32[]{:S(2)}, u32[]{:S(2)}) async-start(bf16[16,3,2048]{2,1,0:T(4,128)(2,1)} %copy.73), calls=%async_computation.3 | async-start | bytes 524288 | tf_op jit(solution)/shard_map/all_to_all | solution.py:104
  110.8 0.0 copy-done.7
  110.8 0.1 fusion.63
  110.9 9.9 %all-to-all-done.3 = bf16[16,3,2048]{2,1,0:T(4,128)(2,1)S(1)} async-done(((bf16[16,3,2048]{2,1,0:T(4,128)(2,1)}), bf16[16,3,2048]{2,1,0:T(4,128)(2,1)S(1)}, u32[]{:S(2)}, u32[]{:S(2)}) %all-to-all-start.3) | async-done | bytes 196640 | tf_op jit(solution)/shard_map/all_to_all | solution.py:104
  120.7 0.1 convert_reduce_fusion
  120.9 0.9 fusion.16
  (15 shorter events, 0.2 us)
Async XLA Ops:
  0.6 25.2 %copy-start = (bf16[2048,128]{1,0:T(8,128)(2,1)S(1)}, bf16[2048,128]{1,0:T(8,128)(2,1)}, u32[]{:S(2)}) copy-start(bf16[2048,128]{1,0:T(8,128)(2,1)} %param.21) | copy-start | bytes 1572868
  28.7 22.7 %copy-start.5 = (f32[128]{0:T(128)S(1)}, f32[128]{0:T(128)}, u32[]{:S(2)}) copy-start(f32[128]{0:T(128)} %param.26) | copy-start | bytes 1540
  30.0 40.0 %copy-start.2 = (bf16[2048,128]{1,0:T(8,128)(2,1)S(1)}, bf16[2048,128]{1,0:T(8,128)(2,1)}, u32[]{:S(2)}) copy-start(bf16[2048,128]{1,0:T(8,128)(2,1)} %param.27) | copy-start | bytes 1572868
  30.7 10.4 %all-to-all-start = ((bf16[4,64,128]{2,0,1:T(4,128)(2,1)}), bf16[4,64,128]{2,0,1:T(4,128)(2,1)S(1)}, u32[]{:S(2)}, u32[]{:S(2)}) async-start(bf16[4,64,128]{2,0,1:T(4,128)(2,1)} %copy.66), calls=%async_computation | async-start | bytes 131072 | tf_op jit(solution)/shard_map/all_to_all | solution.py:73
  41.1 39.7 %copy-start.3 = (bf16[4,2048]{1,0:T(4,128)(2,1)S(1)}, bf16[4,2048]{1,0:T(4,128)(2,1)}, u32[]{:S(2)}) copy-start(bf16[4,2048]{1,0:T(4,128)(2,1)} %param.16) | copy-start | bytes 49156
  41.1 39.8 %copy-start.6 = (f32[2048]{0:T(1024)S(1)}, f32[2048]{0:T(1024)}, u32[]{:S(2)}) copy-start(f32[2048]{0:T(1024)} %param.28) | copy-start | bytes 24580
  45.6 2.0 %copy-start.1 = (f32[4,16,128,128]{3,2,1,0:T(8,128)}, f32[4,16,128,128]{3,2,1,0:T(8,128)S(1)}, u32[]{:S(2)}) copy-start(f32[4,16,128,128]{3,2,1,0:T(8,128)S(1)} %multiply_add_fusion) | copy-start | bytes 12582916
  70.8 10.0 %all-to-all-start.1 = ((bf16[16,4,128]{2,1,0:T(4,128)(2,1)}), bf16[16,4,128]{2,1,0:T(4,128)(2,1)S(1)}, u32[]{:S(2)}, u32[]{:S(2)}) async-start(bf16[16,4,128]{2,1,0:T(4,128)(2,1)} %bitcast.21), calls=%async_computation.1 | async-start | bytes 32768 | tf_op jit(solution)/shard_map/all_to_all | solution.py:78
  98.4 12.3 %copy-start.7 = (bf16[4,2]{0,1:T(2,128)(2,1)S(1)}, bf16[4,2]{0,1:T(2,128)(2,1)}, u32[]{:S(2)}) copy-start(bf16[4,2]{0,1:T(2,128)(2,1)} %param.19) | copy-start | bytes 52
  98.5 12.3 %copy-start.4 = (s32[4,2]{0,1:T(2,128)S(1)}, s32[4,2]{0,1:T(2,128)}, u32[]{:S(2)}) copy-start(s32[4,2]{0,1:T(2,128)} %param.18) | copy-start | bytes 100
  107.2 13.5 %all-to-all-start.3 = ((bf16[16,3,2048]{2,1,0:T(4,128)(2,1)}), bf16[16,3,2048]{2,1,0:T(4,128)(2,1)S(1)}, u32[]{:S(2)}, u32[]{:S(2)}) async-start(bf16[16,3,2048]{2,1,0:T(4,128)(2,1)} %copy.73), calls=%async_computation.3 | async-start | bytes 524288 | tf_op jit(solution)/shard_map/all_to_all | solution.py:104
where the time goes:
time: 123 us; the launch traced here: 122 us
  blocking collectives  55.2 us (45%)
  matrix products  22.1 us (18%)
  waiting for transfers between devices  21.7 us (18%)
  starting transfers between devices  10.5 us (9%)
  other arithmetic  7.51 us (6%)
  local copies, waits for them, and re-layouts  3.88 us (3%)
    all_gather x1, blocking collectives, local(): lax.all_gather(tokens, 'ep', axis=0, tiled=True)  24.2 us
    all_gather x1, blocking collectives, local(): lax.all_gather(mixed, 'ep', axis=0, tiled=True)  18.4 us
    all_to_all x1, blocking collectives, local(): lax.all_to_all(outgoing, 'ep', split_axis=0, concat_axis=0, tiled=True)  12.6 us
    all_to_all x1, waiting for transfers between devices, local(): lax.all_to_all(partial_rows.astype(jnp.bfloat16), 'ep', split_axis=0, con...  9.86 us
    dot_general x1, matrix products, local(): jnp.einsum('scf,fd->scd', hidden, expert_down, preferred_element_type=jnp...  7.88 us
    all_to_all x1, waiting for transfers between devices, local(): lax.all_to_all(mixer_cols, 'ep', split_axis=0, concat_axis=1, tiled=True)  6.45 us
    all_to_all x1, waiting for transfers between devices, local(): lax.all_to_all(projected, 'ep', split_axis=1, concat_axis=2, tiled=True)  5.34 us
    dot_general x1, matrix products, local(): jnp.einsum('scd,df->scf', arrived, expert_gate, preferred_element_type=jn...  4.49 us
  transfers between devices with their start and end apart: 3, of which 3 were waited for; matrix products, arithmetic and copies ran while one was open for 1% of the time, Pallas kernels for 0%

commit v1 on v0

--- a/solution.py
+++ b/solution.py
@@ -75,7 +75,10 @@
     mixer_cols = jnp.dot(
         lax.all_gather(mixed, "ep", axis=0, tiled=True), w_out, preferred_element_type=jnp.float32
     ).astype(jnp.bfloat16)
-    mixer_rows = lax.all_to_all(mixer_cols, "ep", split_axis=0, concat_axis=1, tiled=True)
+    mixer_rows = jnp.concatenate(
+        lax.all_to_all(jnp.stack(jnp.split(mixer_cols, lax.axis_size("ep"), axis=0)), "ep", 0, 0),
+        axis=1,
+    )
     middle = tokens.astype(jnp.float32) + mixer_rows.astype(jnp.float32)
     normed_two = rms_scale(middle, norm_ffn).astype(jnp.bfloat16)
     matches = (route_ids[:, :, None] == jnp.arange(EXPERTS, dtype=jnp.int32)[None, None, :]).astype(

time: 123 us -> 131 us (1.065)
  local copies, waits for them, and re-layouts: 3.88 us -> 12.9 us
    unnamed x18 -> x33, local copies, waits for them, and re-layouts: 2.13 us -> 10.6 us
where the time goes in v1:
time: 131 us; the launch traced here: 130 us
  blocking collectives  55.2 us (42%)
  waiting for transfers between devices  21.7 us (17%)
  matrix products  21.5 us (16%)
  local copies, waits for them, and re-layouts  12.9 us (10%)
  starting transfers between devices  10.5 us (8%)
  other arithmetic  7.51 us (6%)
    all_gather x1, blocking collectives, local(): lax.all_gather(tokens, 'ep', axis=0, tiled=True)  24.2 us
    all_gather x1, blocking collectives, local(): lax.all_gather(mixed, 'ep', axis=0, tiled=True)  18.4 us
    all_to_all x1, blocking collectives, local(): lax.all_to_all(outgoing, 'ep', split_axis=0, concat_axis=0, tiled=True)  12.6 us
    unnamed x33, local copies, waits for them, and re-layouts  10.6 us
    all_to_all x1, waiting for transfers between devices, local(): lax.all_to_all(partial_rows.astype(jnp.bfloat16), 'ep', split_axis=0, con...  9.86 us
    dot_general x1, matrix products, local(): jnp.einsum('scf,fd->scd', hidden, expert_down, preferred_element_type=jnp...  7.88 us
    all_to_all x1, waiting for transfers between devices, local(): lax.all_to_all(jnp.stack(jnp.split(mixer_cols, lax.axis_size('ep'), axis=...  6.45 us
    all_to_all x1, waiting for transfers between devices, local(): lax.all_to_all(projected, 'ep', split_axis=1, concat_axis=2, tiled=True)  5.34 us
  transfers between devices with their start and end apart: 3, of which 3 were waited for; matrix products, arithmetic and copies ran while one was open for 1% of the time, Pallas kernels for 0%

profile of v1, /device:TPU:0, one launch (start us, length us, event | category | flops | bytes accessed | tf_op | source)
XLA Modules:
  0.0 130.2 jit_solution(10254236916201537277)
XLA Ops:
  0.6 24.2 %all-gather = bf16[16,4,2048]{2,1,0:T(4,128)(2,1)S(1)} all-gather(bf16[1,4,2048]{2,1,0:T(4,128)(2,1)} %bitcast.201), channel_id=1, replica_groups=mesh['grp'=2,'ep'=16] {'ep'}, dimensions={0}, use_global_device_ids=true | all-gather | bytes 278528 | tf_op jit(solution)/shard_map/all_gather | solution.py:62
  24.9 0.1 multiply_reduce_fusion
  25.0 0.8 multiply_convert_fusion
  25.9 0.2 fusion.17
  26.1 1.3 fusion.18
  27.4 1.3 fusion.19
  28.7 1.3 fusion.20
  30.0 0.7 copy.66
  30.7 3.5 %all-to-all-start = ((bf16[4,64,128]{2,0,1:T(4,128)(2,1)}), bf16[4,64,128]{2,0,1:T(4,128)(2,1)S(1)}, u32[]{:S(2)}, u32[]{:S(2)}) async-start(bf16[4,64,128]{2,0,1:T(4,128)(2,1)} %copy.66), calls=%async_computation | async-start | bytes 131072 | tf_op jit(solution)/shard_map/all_to_all | solution.py:73
  34.2 0.7 log_bitcast_fusion
  34.9 0.8 convert_reduce_fusion.1
  35.7 5.3 %all-to-all-done = bf16[4,64,128]{2,0,1:T(4,128)(2,1)S(1)} async-done(((bf16[4,64,128]{2,0,1:T(4,128)(2,1)}), bf16[4,64,128]{2,0,1:T(4,128)(2,1)S(1)}, u32[]{:S(2)}, u32[]{:S(2)}) %all-to-all-start) | async-done | bytes 65568 | tf_op jit(solution)/shard_map/all_to_all | solution.py:73
  41.2 4.4 %multiply_add_fusion = f32[4,16,128,128]{3,2,1,0:T(8,128)S(1)} fusion(f32[4,16,128,128]{3,2,1,0:T(8,128)} %param.17, f32[4,16,128]{2,1,0:T(8,128)S(1)} %fusion.57, f32[4,16,128]{2,1,0:T(8,128)S(1)} %get-tuple-element.3, f32[4,16,128]{2,1,0:T(8,128)S(1)} %get-tuple-element.2), kind=kLoop, calls=%fused_computation.6 | loop fusion | flops 3145728 | bytes 8486912 | tf_op jit(solution)/shard_map/add | solution.py:31
  45.6 2.0 %copy-done.1 = f32[4,16,128,128]{3,2,1,0:T(8,128)} copy-done((f32[4,16,128,128]{3,2,1,0:T(8,128)}, f32[4,16,128,128]{3,2,1,0:T(8,128)S(1)}, u32[]{:S(2)}) %copy-start.1) | copy-done | bytes 4194328
  47.6 3.6 %fusion.73 = f32[4,16,1,128]{3,2,1,0:T(1,128)S(1)} fusion(f32[4,16,128,1]{2,3,1,0:T(1,128)S(1)} %bitcast.200, f32[4,16,128,128]{3,2,1,0:T(8,128)S(1)} %multiply_add_fusion), kind=kOutput, calls=%fused_computation.135 | convolution fusion | flops 12582912 | bytes 4259840 | tf_op jit(solution)/shard_map/thk,thkv->thv/dot_general | solution.py:34
  51.3 0.1 multiply_reduce_fusion.2
  51.5 18.4 %all-gather.1 = bf16[16,4,2048]{2,1,0:T(4,128)(2,1)S(1)} all-gather(bf16[1,4,2048]{2,1,0:T(4,128)(2,1)S(1)} %reshape.163), channel_id=1, replica_groups=mesh['grp'=2,'ep'=16] {'ep'}, dimensions={0}, use_global_device_ids=true | all-gather | bytes 278528 | tf_op jit(solution)/shard_map/all_gather | solution.py:76
  70.0 0.2 convolution_convert_fusion.1
  70.2 0.6 constant_dynamic-update-slice_fusion.15
  70.8 0.6 constant_dynamic-update-slice_fusion.14
  71.3 0.6 constant_dynamic-update-slice_fusion.13
  71.9 0.6 constant_dynamic-update-slice_fusion.12
  72.5 0.6 constant_dynamic-update-slice_fusion.11
  73.0 0.6 constant_dynamic-update-slice_fusion.10
  73.6 0.6 constant_dynamic-update-slice_fusion.9
  74.2 0.6 constant_dynamic-update-slice_fusion.8
  74.7 0.6 constant_dynamic-update-slice_fusion.7
  75.3 0.6 constant_dynamic-update-slice_fusion.6
  75.9 0.6 constant_dynamic-update-slice_fusion.5
  76.4 0.6 constant_dynamic-update-slice_fusion.4
  77.0 0.6 constant_dynamic-update-slice_fusion.3
  77.5 0.6 constant_dynamic-update-slice_fusion.2
  78.1 0.6 constant_dynamic-update-slice_fusion.1
  78.7 0.6 constant_dynamic-update-slice_fusion
  79.2 3.5 %all-to-all-start.1 = ((bf16[16,4,128]{2,1,0:T(4,128)(2,1)}), bf16[16,4,128]{2,1,0:T(4,128)(2,1)S(1)}, u32[]{:S(2)}, u32[]{:S(2)}) async-start(bf16[16,4,128]{2,1,0:T(4,128)(2,1)} %constant_dynamic-update-slice_fusion), calls=%async_computation.1 | async-start | bytes 32768 | tf_op jit(solution)/shard_map/all_to_all | solution.py:79
  82.8 6.5 %all-to-all-done.1 = bf16[16,4,128]{2,1,0:T(4,128)(2,1)S(1)} async-done(((bf16[16,4,128]{2,1,0:T(4,128)(2,1)}), bf16[16,4,128]{2,1,0:T(4,128)(2,1)S(1)}, u32[]{:S(2)}, u32[]{:S(2)}) %all-to-all-start.1) | async-done | bytes 16416 | tf_op jit(solution)/shard_map/all_to_all | solution.py:79
  89.2 0.1 multiply_reduce_fusion.1
  89.4 0.2 convolution_convert_fusion
  89.7 0.1 broadcast_in_dim.2
  89.8 12.6 %all_to_all.30 = bf16[16,3,2048]{2,1,0:T(4,128)(2,1)S(1)} all-to-all(bf16[16,3,2048]{2,1,0:T(4,128)(2,1)S(1)} %bitcast.193), channel_id=1, replica_groups=mesh['grp'=2,'ep'=16] {'ep'}, dimensions={0} | all-to-all | bytes 393216 | tf_op jit(solution)/shard_map/all_to_all | solution.py:100
  102.4 4.5 %fusion.4 = f32[16,3,1792]{2,0,1:T(8,128)S(1)} fusion(bf16[2048,1792]{1,0:T(8,128)(2,1)} %param.29, bf16[16,3,2048]{2,1,0:T(4,128)(2,1)S(1)} %all_to_all.30), kind=kOutput, calls=%fused_computation.4 | convolution fusion | flops 352321536 | bytes 7880704 | tf_op jit(solution)/shard_map/scd,df->scf/dot_general | solution.py:101
  106.9 7.9 %fusion.12 = bf16[16,3,2048]{2,0,1:T(8,128)(2,1)S(1)} fusion(bf16[1792,2048]{1,0:T(8,128)(2,1)} %param.31, bf16[2048,1792]{1,0:T(8,128)(2,1)} %param.30, f32[16,3,1792]{2,0,1:T(8,128)S(1)} %fusion.4, bf16[16,3,2048]{2,1,0:T(4,128)(2,1)S(1)} %all_to_all.30), kind=kOutput, calls=%fused_computation.9 | convolution fusion | flops 705257472 | bytes 15417344 | tf_op jit(solution)/shard_map/scf,fd->scd/dot_general | solution.py:104
  114.8 0.9 copy.73
  115.7 3.5 %all-to-all-start.3 = ((bf16[16,3,2048]{2,1,0:T(4,128)(2,1)}), bf16[16,3,2048]{2,1,0:T(4,128)(2,1)S(1)}, u32[]{:S(2)}, u32[]{:S(2)}) async-start(bf16[16,3,2048]{2,1,0:T(4,128)(2,1)} %copy.73), calls=%async_computation.3 | async-start | bytes 524288 | tf_op jit(solution)/shard_map/all_to_all | solution.py:107
  119.2 0.1 fusion.63
  119.3 9.9 %all-to-all-done.3 = bf16[16,3,2048]{2,1,0:T(4,128)(2,1)S(1)} async-done(((bf16[16,3,2048]{2,1,0:T(4,128)(2,1)}), bf16[16,3,2048]{2,1,0:T(4,128)(2,1)S(1)}, u32[]{:S(2)}, u32[]{:S(2)}) %all-to-all-start.3) | async-done | bytes 196640 | tf_op jit(solution)/shard_map/all_to_all | solution.py:107
  129.2 0.1 convert_reduce_fusion
  129.3 0.9 fusion.16
  (31 shorter events, 0.5 us)
Async XLA Ops:
  0.6 25.2 %copy-start = (bf16[2048,128]{1,0:T(8,128)(2,1)S(1)}, bf16[2048,128]{1,0:T(8,128)(2,1)}, u32[]{:S(2)}) copy-start(bf16[2048,128]{1,0:T(8,128)(2,1)} %param.21) | copy-start | bytes 1572868
  28.7 22.7 %copy-start.5 = (f32[128]{0:T(128)S(1)}, f32[128]{0:T(128)}, u32[]{:S(2)}) copy-start(f32[128]{0:T(128)} %param.26) | copy-start | bytes 1540
  30.0 40.0 %copy-start.2 = (bf16[2048,128]{1,0:T(8,128)(2,1)S(1)}, bf16[2048,128]{1,0:T(8,128)(2,1)}, u32[]{:S(2)}) copy-start(bf16[2048,128]{1,0:T(8,128)(2,1)} %param.27) | copy-start | bytes 1572868
  30.7 10.4 %all-to-all-start = ((bf16[4,64,128]{2,0,1:T(4,128)(2,1)}), bf16[4,64,128]{2,0,1:T(4,128)(2,1)S(1)}, u32[]{:S(2)}, u32[]{:S(2)}) async-start(bf16[4,64,128]{2,0,1:T(4,128)(2,1)} %copy.66), calls=%async_computation | async-start | bytes 131072 | tf_op jit(solution)/shard_map/all_to_all | solution.py:73
  41.1 48.1 %copy-start.3 = (bf16[4,2048]{1,0:T(4,128)(2,1)S(1)}, bf16[4,2048]{1,0:T(4,128)(2,1)}, u32[]{:S(2)}) copy-start(bf16[4,2048]{1,0:T(4,128)(2,1)} %param.16) | copy-start | bytes 49156
  41.2 48.2 %copy-start.6 = (f32[2048]{0:T(1024)S(1)}, f32[2048]{0:T(1024)}, u32[]{:S(2)}) copy-start(f32[2048]{0:T(1024)} %param.28) | copy-start | bytes 24580
  45.6 2.0 %copy-start.1 = (f32[4,16,128,128]{3,2,1,0:T(8,128)}, f32[4,16,128,128]{3,2,1,0:T(8,128)S(1)}, u32[]{:S(2)}) copy-start(f32[4,16,128,128]{3,2,1,0:T(8,128)S(1)} %multiply_add_fusion) | copy-start | bytes 12582916
  79.2 10.0 %all-to-all-start.1 = ((bf16[16,4,128]{2,1,0:T(4,128)(2,1)}), bf16[16,4,128]{2,1,0:T(4,128)(2,1)S(1)}, u32[]{:S(2)}, u32[]{:S(2)}) async-start(bf16[16,4,128]{2,1,0:T(4,128)(2,1)} %constant_dynamic-update-slice_fusion), calls=%async_computation.1 | async-start | bytes 32768 | tf_op jit(solution)/shard_map/all_to_all | solution.py:79
  106.9 12.3 %copy-start.7 = (bf16[4,2]{0,1:T(2,128)(2,1)S(1)}, bf16[4,2]{0,1:T(2,128)(2,1)}, u32[]{:S(2)}) copy-start(bf16[4,2]{0,1:T(2,128)(2,1)} %param.19) | copy-start | bytes 52
  106.9 12.3 %copy-start.4 = (s32[4,2]{0,1:T(2,128)S(1)}, s32[4,2]{0,1:T(2,128)}, u32[]{:S(2)}) copy-start(s32[4,2]{0,1:T(2,128)} %param.18) | copy-start | bytes 100
  115.7 13.5 %all-to-all-start.3 = ((bf16[16,3,2048]{2,1,0:T(4,128)(2,1)}), bf16[16,3,2048]{2,1,0:T(4,128)(2,1)S(1)}, u32[]{:S(2)}, u32[]{:S(2)}) async-start(bf16[16,3,2048]{2,1,0:T(4,128)(2,1)} %copy.73), calls=%async_computation.3 | async-start | bytes 524288 | tf_op jit(solution)/shard_map/all_to_all | solution.py:107
